TPU v7x, 32 devices: a whole 2x2x4 slice. The times are simulated.
32 devices in a mesh: sp: 16 (over z, y, x), tp: 2 (over core).
Axes of the slice: x: 2, y: 2, z: 4, core: 2. Of those that a mesh axis runs over, the one named last changes fastest.
Arguments:
- hidden_in: bfloat16 [4096, 2048], P('sp', 'tp'), may hold values from -6 to 6
- w_query_rec: bfloat16 [2048, 2048], P('sp', 'tp'), may hold values from -0.125 to 0.125
- w_forget: bfloat16 [2048, 2048], P('sp', 'tp'), may hold values from -0.125 to 0.125
- w_input: bfloat16 [2048, 2048], P('sp', 'tp'), may hold values from -0.125 to 0.125
- forget_gap: float32 [2048], P('tp'), may hold values from 1e-05 to 0.08
- decay_extra: float32 [4096, 16], P('sp', 'tp'), may hold values from -0.75 to 0
- rec_gain: float32 [128], replicated, may hold values from 0.1 to 1.9
- w_q_down: bfloat16 [2048, 512], P(None, 'tp'), may hold values from -0.125 to 0.125
- w_kv_down: bfloat16 [2048, 256], P(None, 'tp'), may hold values from -0.125 to 0.125
- w_key_rope: bfloat16 [2048, 32], replicated, may hold values from -0.125 to 0.125
- q_gain: float32 [512], replicated, may hold values from 1.4 to 7
- kv_gain: float32 [256], replicated, may hold values from 1.4 to 7
- w_q_nope: bfloat16 [512, 1024], P(None, 'tp'), may hold values from -0.25 to 0.25
- w_q_rope: bfloat16 [512, 512], P(None, 'tp'), may hold values from -0.25 to 0.25
- w_k_up: bfloat16 [256, 1024], P(None, 'tp'), may hold values from -0.375 to 0.375
- w_v_up: bfloat16 [256, 1024], P(None, 'tp'), may hold values from -0.375 to 0.375
- w_out_rec: bfloat16 [2048, 2048], P('tp'), may hold values from -0.109375 to 0.109375
- w_out_att: bfloat16 [1024, 2048], P('tp'), may hold values from -0.109375 to 0.109375
Outputs:
- mixed_out: bfloat16 [4096, 2048], P(('sp', 'tp'))
All inputs are finite; a program needn't handle non-finite values.
Results may differ from a plain program's by a relative error of at most 0.02.
The roundings to bfloat16 on the way count: a program that leaves them out, or rounds other values in their place, can miss the bound.
Values may be sent and summed in bfloat16 or wider, within the bound.
A program may use at most 128 MiB of HBM per device.

v0:
```python
import math
import jax
import jax.numpy as jnp
from jax import lax
from jax.sharding import PartitionSpec as P

HG_KDIM = 128
HG_VDIM = 128
HG_BLOCK = 64
NOPE = 64
ROPE = 32
MLA_V = 64
NORM_EPS = 1e-06
ROPE_BASE = 10000.0
NEG_BIG = -1e30


def carried_in(part, axis, combine, identity):
    place = lax.axis_index(axis)
    gathered = jax.tree.map(lambda a: lax.all_gather(a, axis), part)
    state = jax.tree.map(lambda a, e: jnp.zeros_like(a) + jnp.asarray(e, a.dtype), part, identity)

    def one(step, state):
        return combine(
            state, jax.tree.map(lambda a: lax.dynamic_index_in_dim(a, step, 0, False), gathered)
        )

    return lax.fori_loop(0, place, one, state)


def rms_scale(values):
    return values * lax.rsqrt(jnp.mean(values * values, axis=-1, keepdims=True) + NORM_EPS)


def rotate_half(values, cosine, sine_table):
    half_width = values.shape[-1] // 2
    lower_half = values[..., :half_width]
    upper_half = values[..., half_width:]
    return jnp.concatenate(
        [
            lower_half * cosine - upper_half * sine_table,
            lower_half * sine_table + upper_half * cosine,
        ],
        axis=-1,
    )


def rotary_tables(row_count, offset, rot_width):
    positions = jnp.arange(row_count, dtype=jnp.float32) + offset
    frequency = 1.0 / ROPE_BASE ** (jnp.arange(0, rot_width, 2, dtype=jnp.float32) / rot_width)
    angles = positions[:, None] * frequency[None, :]
    return (jnp.cos(angles), jnp.sin(angles))


def block_step(rec_state, inputs):
    queries, key_in, values, log_forget = inputs
    cumulative = jnp.cumsum(log_forget, axis=1)
    log_gaps = cumulative[:, :, None, :] - cumulative[:, None, :, :]
    block_len = queries.shape[1]
    lower_mask = jnp.tril(jnp.ones((block_len, block_len), jnp.float32))
    decays = jnp.exp(jnp.minimum(log_gaps, 0.0)) * lower_mask[None, :, :, None]
    scores = jnp.einsum(
        "htsd,hsd->hts", queries[:, :, None, :] * decays, key_in, precision=lax.Precision.HIGHEST
    )
    block_out = jnp.einsum(
        "hts,hsv->htv", scores, values, precision=lax.Precision.HIGHEST
    ) + jnp.einsum(
        "htd,hdv->htv", queries * jnp.exp(cumulative), rec_state, precision=lax.Precision.HIGHEST
    )
    last_cumul = cumulative[:, -1:, :]
    rec_state = jnp.exp(last_cumul[:, 0, :])[..., None] * rec_state + jnp.einsum(
        "hsd,hsv->hdv",
        key_in * jnp.exp(last_cumul - cumulative),
        values,
        precision=lax.Precision.HIGHEST,
    )
    return (rec_state, block_out)


def score_block(q_nope, q_rope, k_nope, k_rope, values, q_start, k_start):
    score_scale = 1.0 / math.sqrt(NOPE + ROPE)
    scores = (
        jnp.einsum("qhd,khd->hqk", q_nope, k_nope, preferred_element_type=jnp.float32)
        + jnp.einsum("qhr,kr->hqk", q_rope, k_rope, preferred_element_type=jnp.float32)
    ) * score_scale
    q_pos = q_start + jnp.arange(q_nope.shape[0], dtype=jnp.int32)
    k_pos = k_start + jnp.arange(k_nope.shape[0], dtype=jnp.int32)
    allowed = k_pos[None, :] <= q_pos[:, None]
    scores = jnp.where(allowed[None], scores, NEG_BIG)
    block_peak = jnp.max(scores, axis=-1)
    weights = jnp.where(allowed[None], jnp.exp(scores - block_peak[..., None]), 0.0)
    block_total = jnp.sum(weights, axis=-1)
    weights16 = weights.astype(jnp.bfloat16)
    block_sum = jnp.einsum("hqk,khv->hqv", weights16, values, preferred_element_type=jnp.float32)
    return (block_peak, block_total, block_sum)


def merge_terms(earlier, later_part):
    top = jnp.maximum(earlier[0], later_part[0])
    old_factor = jnp.exp(earlier[0] - top)
    new_factor = jnp.exp(later_part[0] - top)
    return (
        top,
        earlier[1] * old_factor + later_part[1] * new_factor,
        earlier[2] * old_factor[..., None] + later_part[2] * new_factor[..., None],
    )


def chain_step(earlier, later_part):
    return (earlier[0] * later_part[0], later_part[0][..., None] * earlier[1] + later_part[1])


def shards(
    hidden_in,
    w_query_rec,
    w_forget,
    w_input,
    forget_gap,
    decay_extra,
    rec_gain,
    w_q_down,
    w_kv_down,
    w_key_rope,
    q_gain,
    kv_gain,
    w_q_nope,
    w_q_rope,
    w_k_up,
    w_v_up,
    w_out_rec,
    w_out_att,
):
    tok_dev = hidden_in.shape[0]
    sp_index = lax.axis_index("sp")
    tp_index = lax.axis_index("tp")
    full_query, full_forget, full_input = (
        lax.all_gather(w_query_rec, "sp", axis=0, tiled=True),
        lax.all_gather(w_forget, "sp", axis=0, tiled=True),
        lax.all_gather(w_input, "sp", axis=0, tiled=True),
    )
    left_weight = jnp.concatenate([full_query, full_forget, full_input], axis=1)
    right_weight = jnp.concatenate([w_q_down, w_kv_down, w_key_rope], axis=1)
    feature_piece = lax.all_gather(hidden_in, "tp", axis=1, tiled=True)
    left_sum = jnp.dot(feature_piece, left_weight, preferred_element_type=jnp.float32)
    right_sum = jnp.dot(feature_piece, right_weight, preferred_element_type=jnp.float32)
    key_cols = full_query.shape[1]
    head_count = key_cols // HG_KDIM
    left_round = left_sum.astype(jnp.bfloat16)
    rec_query = left_round[:, :key_cols].astype(jnp.float32).reshape(tok_dev, head_count, HG_KDIM)
    forget_pre = (
        left_round[:, key_cols : 2 * key_cols]
        .astype(jnp.float32)
        .reshape(tok_dev, head_count, HG_KDIM)
    )
    rec_value = (
        left_round[:, 2 * key_cols :].astype(jnp.float32).reshape(tok_dev, head_count, HG_VDIM)
    )
    gap_rows = forget_gap.reshape(head_count, HG_KDIM)
    closing = jax.nn.sigmoid(-forget_pre)
    key_in = gap_rows * closing
    log_forget = jnp.log1p(-gap_rows * closing) + decay_extra[:, :, None]
    block_count = tok_dev // HG_BLOCK

    def to_blocks(tensor):
        return tensor.reshape(block_count, HG_BLOCK, head_count, tensor.shape[-1]).transpose(
            0, 2, 1, 3
        )

    zero_state = jnp.zeros((head_count, HG_KDIM, HG_VDIM), jnp.float32)
    local_state, local_out = lax.scan(
        block_step,
        zero_state,
        (to_blocks(rec_query), to_blocks(key_in), to_blocks(rec_value), to_blocks(log_forget)),
    )
    local_out = local_out.transpose(0, 2, 1, 3).reshape(tok_dev, head_count, HG_VDIM)
    cumulative = jnp.cumsum(log_forget, axis=0)
    device_decay = jnp.exp(cumulative[-1])
    scanned = carried_in(
        (device_decay, local_state),
        "sp",
        chain_step,
        (jnp.ones_like(device_decay), jnp.zeros_like(local_state)),
    )
    into_state = scanned[1]
    rec_raw = local_out + jnp.einsum(
        "thd,hdv->thv", rec_query * jnp.exp(cumulative), into_state, precision=lax.Precision.HIGHEST
    )
    rec_out = (
        (rms_scale(rec_raw) * rec_gain).astype(jnp.bfloat16).reshape(tok_dev, head_count * HG_VDIM)
    )
    q_cols = w_q_down.shape[1]
    kv_cols = w_kv_down.shape[1]
    right_round = right_sum.astype(jnp.bfloat16)
    q_part = right_round[:, :q_cols]
    kv_part = right_round[:, q_cols : q_cols + kv_cols]
    rope_raw = right_sum[:, q_cols + kv_cols :]
    q_part32 = q_part.astype(jnp.float32)
    kv_part32 = kv_part.astype(jnp.float32)
    square_sums = lax.psum(
        (jnp.sum(q_part32 * q_part32, axis=1), jnp.sum(kv_part32 * kv_part32, axis=1)), "tp"
    )
    q_gain_part = lax.dynamic_slice_in_dim(q_gain, tp_index * q_cols, q_cols, 0)
    kv_gain_part = lax.dynamic_slice_in_dim(kv_gain, tp_index * kv_cols, kv_cols, 0)
    q_norm_part = (
        q_part32 * lax.rsqrt(square_sums[0][:, None] / q_gain.shape[0] + NORM_EPS) * q_gain_part
    ).astype(jnp.bfloat16)
    kv_norm_part = (
        kv_part32 * lax.rsqrt(square_sums[1][:, None] / kv_gain.shape[0] + NORM_EPS) * kv_gain_part
    ).astype(jnp.bfloat16)
    q_normed, latent = (
        lax.all_gather(q_norm_part, "tp", axis=1, tiled=True),
        lax.all_gather(kv_norm_part, "tp", axis=1, tiled=True),
    )
    q_start = sp_index * tok_dev
    cosine, sine_table = rotary_tables(tok_dev, q_start.astype(jnp.float32), ROPE)
    key_rope = rotate_half(rope_raw, cosine, sine_table).astype(jnp.bfloat16)
    att_heads = w_q_nope.shape[1] // NOPE
    q_nope = jnp.dot(q_normed, w_q_nope, preferred_element_type=jnp.float32).astype(jnp.bfloat16)
    q_nope = q_nope.reshape(tok_dev, att_heads, NOPE)
    q_rope = jnp.dot(q_normed, w_q_rope, preferred_element_type=jnp.float32).reshape(
        tok_dev, att_heads, ROPE
    )
    q_rope = rotate_half(q_rope, cosine[:, None, :], sine_table[:, None, :]).astype(jnp.bfloat16)

    def attend(running, latent_rows, rope_rows, key_start):

        def compute(previous):
            k_nope = jnp.dot(latent_rows, w_k_up, preferred_element_type=jnp.float32).astype(
                jnp.bfloat16
            )
            att_value = jnp.dot(latent_rows, w_v_up, preferred_element_type=jnp.float32).astype(
                jnp.bfloat16
            )
            partials = score_block(
                q_nope,
                q_rope,
                k_nope.reshape(-1, att_heads, NOPE),
                rope_rows,
                att_value.reshape(-1, att_heads, MLA_V),
                q_start,
                key_start,
            )
            return merge_terms(previous, partials)

        return lax.cond(key_start <= q_start, compute, lambda previous: previous, running)

    initial_att = (
        jnp.full((att_heads, tok_dev), NEG_BIG, jnp.float32),
        jnp.zeros((att_heads, tok_dev), jnp.float32),
        jnp.zeros((att_heads, tok_dev, MLA_V), jnp.float32),
    )
    latent_piece = lax.all_gather(latent, "sp", axis=0, tiled=True)
    rope_piece = lax.all_gather(key_rope, "sp", axis=0, tiled=True)

    def visit(block_index, current):
        first_row = block_index * tok_dev
        return attend(
            current,
            lax.dynamic_slice_in_dim(latent_piece, first_row, tok_dev, 0),
            lax.dynamic_slice_in_dim(rope_piece, first_row, tok_dev, 0),
            first_row,
        )

    top, total_w, accum = lax.fori_loop(0, latent_piece.shape[0] // tok_dev, visit, initial_att)
    att_out = (accum / total_w[..., None]).transpose(1, 0, 2).reshape(tok_dev, att_heads * MLA_V)
    att_out = att_out.astype(jnp.bfloat16)
    return lax.psum_scatter(
        (
            jnp.dot(rec_out, w_out_rec, preferred_element_type=jnp.float32)
            + jnp.dot(att_out, w_out_att, preferred_element_type=jnp.float32)
        ).astype(jnp.bfloat16),
        "tp",
        scatter_dimension=0,
        tiled=True,
    )


def solution(mesh):
    placed = (
        P("sp", "tp"),
        P("sp", "tp"),
        P("sp", "tp"),
        P("sp", "tp"),
        P("tp"),
        P("sp", "tp"),
        P(),
        P(None, "tp"),
        P(None, "tp"),
        P(),
        P(),
        P(),
        P(None, "tp"),
        P(None, "tp"),
        P(None, "tp"),
        P(None, "tp"),
        P("tp", None),
        P("tp", None),
    )
    return jax.shard_map(
        shards, mesh=mesh, in_specs=placed, out_specs=P(("sp", "tp"), None), check_vma=False
    )
```

profile of v0, /device:TPU:0, one launch (start us, length us, event | category | flops | bytes accessed | tf_op | source)
XLA Modules:
  0.0 698.6 jit_solution(387113204665993834)
XLA Ops:
  11.5 9.2 %all-gather.14.cloned.1.call-done = bf16[256,2048]{1,0:T(8,128)(2,1)} async-done(((bf16[256,1024]{1,0:T(8,128)(2,1)}), bf16[256,2048]{1,0:T(8,128)(2,1)}) %all-gather.14.cloned.1.call-update) | async-done | bytes 1048592 | tf_op jit(solution)/shard_map/all_gather | solution.py:143
  20.7 3.2 fusion.75
  23.9 3.0 all-reduce
  29.2 71.0 %all-gather.8.cloned.1.call-done = bf16[2048,1024]{1,0:T(8,128)(2,1)} async-done(((bf16[128,1024]{1,0:T(8,128)(2,1)}), bf16[2048,1024]{1,0:T(8,128)(2,1)}) %all-gather.8.cloned.1.call-update) | async-done | bytes 4194320 | tf_op jit(solution)/shard_map/all_gather | solution.py:137
  100.2 77.0 %all-gather.10.cloned.1.call-done = bf16[2048,1024]{1,0:T(8,128)(2,1)} async-done(((bf16[128,1024]{1,0:T(8,128)(2,1)}), bf16[2048,1024]{1,0:T(8,128)(2,1)}) %all-gather.10.cloned.1.call-update) | async-done | bytes 4194320 | tf_op jit(solution)/shard_map/all_gather | solution.py:138
  177.2 76.8 %all-gather.12.cloned.1.call-done = bf16[2048,1024]{1,0:T(8,128)(2,1)} async-done(((bf16[128,1024]{1,0:T(8,128)(2,1)}), bf16[2048,1024]{1,0:T(8,128)(2,1)}) %all-gather.12.cloned.1.call-update) | async-done | bytes 4194320 | tf_op jit(solution)/shard_map/all_gather | solution.py:139
  254.1 6.9 fusion.43
  281.4 164.5 %while.44 = (s32[]{:T(128)}, f32[8,128,128]{2,1,0:T(8,128)S(1)}, f32[4,8,64,128]{3,1,2,0:T(8,128)}, f32[4,8,64,128]{3,1,2,0:T(8,128)}, f32[4,8,64,128]{3,1,2,0:T...) while((s32[]{:T(128)}, f32[8,128,128]{2,1,0:T(8,128)S(1)}, ...), condition=%wide.region_2.3_spmd.clone, body=%wide.region_0.2_spmd.clone.sunk | while | flops 323690496 | bytes 42786940 | solution.py:170
  284.9 3.6 multiply_multiply_fusion.2
  288.6 30.8 %fusion.122 = f32[8,64,1,64]{3,2,1,0:T(1,128)S(1)} fusion(f32[8,64,64,128]{3,2,1,0:T(8,128)S(1)} %multiply_multiply_fusion.2, f32[8,64,128,1]{2,0,1,3:T(8,128)S(1)} %get-tuple-element.728), kind=kOutput, calls=%fused_computation.29.clone.1 | convolution fusion | flops 50331648 | bytes 17170432 | tf_op jit(solution)/shard_map/while/body/eval_jaxpr/htsd,hsd->hts/dot_general | solution.py:62
  326.0 3.6 multiply_multiply_fusion.2
  329.6 30.8 %fusion.122 = f32[8,64,1,64]{3,2,1,0:T(1,128)S(1)} fusion(f32[8,64,64,128]{3,2,1,0:T(8,128)S(1)} %multiply_multiply_fusion.2, f32[8,64,128,1]{2,0,1,3:T(8,128)S(1)} %get-tuple-element.728), kind=kOutput, calls=%fused_computation.29.clone.1 | convolution fusion | flops 50331648 | bytes 17170432 | tf_op jit(solution)/shard_map/while/body/eval_jaxpr/htsd,hsd->hts/dot_general | solution.py:62
  367.1 3.6 multiply_multiply_fusion.2
  370.7 30.8 %fusion.122 = f32[8,64,1,64]{3,2,1,0:T(1,128)S(1)} fusion(f32[8,64,64,128]{3,2,1,0:T(8,128)S(1)} %multiply_multiply_fusion.2, f32[8,64,128,1]{2,0,1,3:T(8,128)S(1)} %get-tuple-element.728), kind=kOutput, calls=%fused_computation.29.clone.1 | convolution fusion | flops 50331648 | bytes 17170432 | tf_op jit(solution)/shard_map/while/body/eval_jaxpr/htsd,hsd->hts/dot_general | solution.py:62
  408.1 3.6 multiply_multiply_fusion.2
  411.8 30.8 %fusion.122 = f32[8,64,1,64]{3,2,1,0:T(1,128)S(1)} fusion(f32[8,64,64,128]{3,2,1,0:T(8,128)S(1)} %multiply_multiply_fusion.2, f32[8,64,128,1]{2,0,1,3:T(8,128)S(1)} %get-tuple-element.728), kind=kOutput, calls=%fused_computation.29.clone.1 | convolution fusion | flops 50331648 | bytes 17170432 | tf_op jit(solution)/shard_map/while/body/eval_jaxpr/htsd,hsd->hts/dot_general | solution.py:62
  453.1 44.3 %all_gather.44 = bf16[4096,32]{0,1:T(8,128)(2,1)} all-gather(bf16[256,32]{0,1:T(8,128)(2,1)S(1)} %pad_maximum_fusion.1), channel_id=1, replica_groups=mesh['sp'=16,'tp'=2] {'sp'}, dimensions={0}, use_global_device_ids=true | all-gather | bytes 278528 | tf_op jit(solution)/shard_map/all_gather | solution.py:253
  497.4 4.1 copy.90
  501.5 7.4 %while.43 = (s32[]{:T(128)}, f32[8,256]{1,0:T(8,128)S(1)}, f32[8,256]{1,0:T(8,128)S(1)}, f32[8,256,64]{1,2,0:T(8,128)S(1)}, s32[]{:T(128)}, /*index=5*/bf16[4096...) while((s32[]{:T(128)}, f32[8,256]{1,0:T(8,128)S(1)}, ...), condition=%wide.region_17.18_spmd, body=%wide.region_12.17_spmd.sunk | while | flops 307962368 | bytes 15733113 | solution.py:264
  501.5 6.7 conditional.2
  522.2 136.0 %all_gather.38 = f32[16,8,128]{2,1,0:T(8,128)S(1)} all-gather(f32[1,8,128]{2,1,0:T(8,128)S(1)} %exp.49), channel_id=1, replica_groups=mesh['sp'=16,'tp'=2] {'sp'}, dimensions={0}, use_global_device_ids=true | all-gather | bytes 69632 | tf_op jit(solution)/shard_map/all_gather | solution.py:20
  658.2 2.9 copy_multiply_fusion
  661.2 3.0 multiply_reduce_fusion
  667.4 24.3 %reduce-scatter.2.cloned.1.call-done = bf16[128,2048]{1,0:T(8,128)(2,1)} async-done(((bf16[256,2048]{1,0:T(8,128)(2,1)}), bf16[128,2048]{1,0:T(8,128)(2,1)}) %reduce-scatter.2.cloned.1.call-update) | async-done | bytes 524304 | tf_op jit(solution)/shard_map/reduce_scatter | solution.py:267
  (176 shorter events, 84.2 us)
Async XLA Ops:
  6.5 659.1 %copy-start = (bf16[512,2048]{1,0:T(8,128)(2,1)S(1)}, bf16[512,2048]{1,0:T(8,128)(2,1)}, u32[]{:S(2)}) copy-start(bf16[512,2048]{1,0:T(8,128)(2,1)} %param.43) | copy-start | bytes 6291460
  6.5 4.9 copy-start.14
  6.5 5.0 copy-start.9
  6.5 14.1 %all-gather.14.cloned.1.call-start = ((), (), s32[]{:S(2)}) async-start(), calls=%async_computation.4 | async-start | bytes 1572864 | tf_op jit(solution)/shard_map/all_gather | solution.py:143
  7.3 93.0 %all-gather.8.cloned.1.call-start = ((), (), s32[]{:S(2)}) async-start(), calls=%async_computation.1 | async-start | bytes 4456448 | tf_op jit(solution)/shard_map/all_gather | solution.py:137
  8.0 169.2 %all-gather.10.cloned.1.call-start = ((), (), s32[]{:S(2)}) async-start(), calls=%async_computation.2 | async-start | bytes 4456448 | tf_op jit(solution)/shard_map/all_gather | solution.py:138
  8.7 245.3 %all-gather.12.cloned.1.call-start = ((), (), s32[]{:S(2)}) async-start(), calls=%async_computation.3 | async-start | bytes 4456448 | tf_op jit(solution)/shard_map/all_gather | solution.py:139
  9.3 488.1 %all-gather.16.cloned.1.call-start = ((), (), s32[]{:S(2)}) async-start(), calls=%async_computation.5 | async-start | bytes 2228224 | tf_op jit(solution)/shard_map/all_gather | solution.py:252
  11.5 268.1 %copy-start.7 = (f32[8,128]{1,0:T(8,128)}, f32[8,128]{1,0:T(8,128)S(1)}, u32[]{:S(2)}) copy-start(f32[8,128]{1,0:T(8,128)S(1)} %bitcast_negate_fusion) | copy-start | bytes 12292
  29.1 631.9 %all-gather.18.cloned.1.call-start = ((), (), s32[]{:S(2)}) async-start(), calls=%async_computation.7 | async-start | bytes 8912896 | tf_op jit(solution)/shard_map/all_gather | solution.py:20
  276.3 1.6 copy-start.4
  276.3 1.9 copy-start.5
  281.3 165.4 %copy-start.8 = (f32[8,128]{1,0:T(8,128)S(1)}, f32[8,128]{1,0:T(8,128)}, u32[]{:S(2)}) copy-start(f32[8,128]{1,0:T(8,128)} %copy-done.7) | copy-start | bytes 12292
  281.3 165.5 %copy-start.12 = (f32[512]{0:T(512)S(1)}, f32[512]{0:T(512)}, u32[]{:S(2)}) copy-start(f32[512]{0:T(512)} %param.36) | copy-start | bytes 6148
  281.3 165.6 %copy-start.10 = (f32[256]{0:T(256)S(1)}, f32[256]{0:T(256)}, u32[]{:S(2)}) copy-start(f32[256]{0:T(256)} %get-tuple-element.540) | copy-start | bytes 3076
  281.3 167.7 %copy-start.6 = (bf16[512,512]{1,0:T(8,128)(2,1)S(1)}, bf16[512,512]{1,0:T(8,128)(2,1)}, u32[]{:S(2)}) copy-start(bf16[512,512]{1,0:T(8,128)(2,1)} %param.38) | copy-start | bytes 1572868
  445.8 0.8 copy-start.1
  446.7 245.1 %reduce-scatter.2.cloned.1.call-start = ((), (), s32[]{:S(2)}) async-start(), calls=%async_computation.6 | async-start | bytes 1572864 | tf_op jit(solution)/shard_map/reduce_scatter | solution.py:267
  504.5 1.5 copy-start.3
  516.2 142.0 %copy-start.2 = (f32[256,1024]{0,1:T(8,128)S(1)}, f32[256,1024]{0,1:T(8,128)}, u32[]{:S(2)}) copy-start(f32[256,1024]{0,1:T(8,128)} %get-tuple-element.554) | copy-start | bytes 3145732
  661.1 3.1 copy-start.11
  661.1 3.2 copy-start.13
Sparse Core Ops, SparseCore 0:
  8.9 11.7 all-gather.13
  23.4 76.7 all-gather.7
  103.0 74.1 all-gather.9
  179.9 74.1 all-gather.11
  256.6 63.3 all-gather.15
  446.8 112.9 all-gather.17
  667.6 24.1 reduce-scatter.1
where the time goes:
time: 702 us; the launch traced here: 699 us
  waiting for transfers between devices  261 us (37%)
  blocking collectives  187 us (27%)
  matrix products  156 us (22%)
  local copies, waits for them, and re-layouts  41.7 us (6%)
  other arithmetic  37 us (5%)
  between operations  13.8 us (2%)
    all_gather x1, blocking collectives, carried_in(): gathered = jax.tree.map(lambda a: lax.all_gather(a, axis), part)  136 us
    dot_general x4, matrix products, block_step(): jnp.einsum('htsd,hsd->hts', queries[:, :, None, :] * decays, key_in, prec...  123 us
    all_gather x1, waiting for transfers between devices, shards(): lax.all_gather(w_forget, 'sp', axis=0, tiled=True)  77 us
    all_gather x1, waiting for transfers between devices, shards(): lax.all_gather(w_input, 'sp', axis=0, tiled=True)  76.8 us
    all_gather x1, waiting for transfers between devices, shards(): lax.all_gather(w_query_rec, 'sp', axis=0, tiled=True)  71 us
    all_gather x1, blocking collectives, shards(): rope_piece = lax.all_gather(key_rope, 'sp', axis=0, tiled=True)  44.3 us
    reduce_scatter x1, waiting for transfers between devices, shards(): lax.psum_scatter((jnp.dot(rec_out, w_out_rec, preferred_element_type=jnp....  24.3 us
    mul x4, other arithmetic, block_step(): queries[:, :, None, :] * decays  14.5 us
  transfers between devices with their start and end apart: 7, of which 5 were waited for; matrix products, arithmetic and copies ran while one was open for 33% of the time, Pallas kernels for 0%

commit v1 on v0

--- a/solution.py
+++ b/solution.py
@@ -13,6 +13,11 @@
 NORM_EPS = 1e-06
 ROPE_BASE = 10000.0
 NEG_BIG = -1e30
+change_leaves = lambda target, panel: jnp.split(
+    lax.all_gather(jnp.concatenate([target, panel], axis=1), "sp", tiled=True, axis=0),
+    [target.shape[1]],
+    axis=1,
+)
 
 
 def carried_in(part, axis, combine, identity):
@@ -249,8 +254,7 @@
         jnp.zeros((att_heads, tok_dev), jnp.float32),
         jnp.zeros((att_heads, tok_dev, MLA_V), jnp.float32),
     )
-    latent_piece = lax.all_gather(latent, "sp", axis=0, tiled=True)
-    rope_piece = lax.all_gather(key_rope, "sp", axis=0, tiled=True)
+    latent_piece, rope_piece = change_leaves(latent, key_rope)
 
     def visit(block_index, current):
         first_row = block_index * tok_dev

time: 702 us -> 665 us (0.947)
  blocking collectives: 187 us -> 146 us
    all_gather x1 -> x0, blocking collectives: 44.3 us -> none  [shards(): rope_piece = lax.all_gather(key_rope, 'sp', axis=0, tiled=True)]
  transfers between devices with their start and end apart: 7 -> 7, of which waited for: 5 -> 5; matrix products, arithmetic and copies ran while one was open for 33% -> 35% of each run, Pallas kernels for 0% -> 0%
where the time goes in v1:
time: 665 us; the launch traced here: 661 us
  waiting for transfers between devices  258 us (39%)
  matrix products  156 us (23%)
  blocking collectives  146 us (22%)
  local copies, waits for them, and re-layouts  47.1 us (7%)
  other arithmetic  38.7 us (6%)
  between operations  13.8 us (2%)
    all_gather x1, blocking collectives, carried_in(): gathered = jax.tree.map(lambda a: lax.all_gather(a, axis), part)  139 us
    dot_general x4, matrix products, block_step(): jnp.einsum('htsd,hsd->hts', queries[:, :, None, :] * decays, key_in, prec...  123 us
    all_gather x1, waiting for transfers between devices, shards(): lax.all_gather(w_forget, 'sp', axis=0, tiled=True)  77 us
    all_gather x1, waiting for transfers between devices, shards(): lax.all_gather(w_input, 'sp', axis=0, tiled=True)  76.8 us
    all_gather x1, waiting for transfers between devices, shards(): lax.all_gather(w_query_rec, 'sp', axis=0, tiled=True)  69.1 us
    reduce_scatter x1, waiting for transfers between devices, shards(): lax.psum_scatter((jnp.dot(rec_out, w_out_rec, preferred_element_type=jnp....  24.3 us
    mul x4, other arithmetic, block_step(): queries[:, :, None, :] * decays  14.5 us
  transfers between devices with their start and end apart: 7, of which 5 were waited for; matrix products, arithmetic and copies ran while one was open for 35% of the time, Pallas kernels for 0%

profile of v1, /device:TPU:0, one launch (start us, length us, event | category | flops | bytes accessed | tf_op | source)
XLA Modules:
  0.0 661.3 jit_solution(6687738025380617596)
XLA Ops:
  12.9 7.8 %all-gather.14.cloned.1.call-done = bf16[256,2048]{1,0:T(8,128)(2,1)} async-done(((bf16[256,1024]{1,0:T(8,128)(2,1)}), bf16[256,2048]{1,0:T(8,128)(2,1)}) %all-gather.14.cloned.1.call-update) | async-done | bytes 1048592 | tf_op jit(solution)/shard_map/all_gather | solution.py:148
  20.7 3.2 fusion.75
  23.9 3.0 all-reduce
  31.2 69.1 %all-gather.8.cloned.1.call-done = bf16[2048,1024]{1,0:T(8,128)(2,1)} async-done(((bf16[128,1024]{1,0:T(8,128)(2,1)}), bf16[2048,1024]{1,0:T(8,128)(2,1)}) %all-gather.8.cloned.1.call-update) | async-done | bytes 4194320 | tf_op jit(solution)/shard_map/all_gather | solution.py:142
  100.2 77.0 %all-gather.10.cloned.1.call-done = bf16[2048,1024]{1,0:T(8,128)(2,1)} async-done(((bf16[128,1024]{1,0:T(8,128)(2,1)}), bf16[2048,1024]{1,0:T(8,128)(2,1)}) %all-gather.10.cloned.1.call-update) | async-done | bytes 4194320 | tf_op jit(solution)/shard_map/all_gather | solution.py:143
  177.2 76.8 %all-gather.12.cloned.1.call-done = bf16[2048,1024]{1,0:T(8,128)(2,1)} async-done(((bf16[128,1024]{1,0:T(8,128)(2,1)}), bf16[2048,1024]{1,0:T(8,128)(2,1)}) %all-gather.12.cloned.1.call-update) | async-done | bytes 4194320 | tf_op jit(solution)/shard_map/all_gather | solution.py:144
  254.1 6.9 %fusion.43 = bf16[256,3072]{0,1:T(8,128)(2,1)S(1)} fusion(bf16[256,2048]{1,0:T(8,128)(2,1)} %all-gather.14.cloned.1.call-done, bf16[2048,1024]{1,0:T(8,128)(2,1)} %all-gather.12.cloned.1.call-done, bf16[2048,1024]{1,0:T(8,128)(2,1)} %all-gather.10.cloned.1.call-done, bf16[2048,1024]{1,0:T(8,128)(2,1)} %all-gather.8.cloned.1.call-done), kind=kOutput, calls=%fused_computation.65 | convolution fusion | flops 3259760640 | bytes 15204352 | tf_op jit(solution)/shard_map/dot_general | solution.py:149
  281.3 164.5 %while.44 = (s32[]{:T(128)}, f32[8,128,128]{2,1,0:T(8,128)S(1)}, f32[4,8,64,128]{3,1,2,0:T(8,128)}, f32[4,8,64,128]{3,1,2,0:T(8,128)}, f32[4,8,64,128]{3,1,2,0:T...) while((s32[]{:T(128)}, f32[8,128,128]{2,1,0:T(8,128)S(1)}, ...), condition=%wide.region_2.3_spmd.clone, body=%wide.region_0.2_spmd.clone.sunk | while | flops 323690496 | bytes 42786940 | solution.py:175
  284.9 3.6 multiply_multiply_fusion.2
  288.5 30.8 %fusion.122 = f32[8,64,1,64]{3,2,1,0:T(1,128)S(1)} fusion(f32[8,64,64,128]{3,2,1,0:T(8,128)S(1)} %multiply_multiply_fusion.2, f32[8,64,128,1]{2,0,1,3:T(8,128)S(1)} %get-tuple-element.728), kind=kOutput, calls=%fused_computation.29.clone.1 | convolution fusion | flops 50331648 | bytes 17170432 | tf_op jit(solution)/shard_map/while/body/eval_jaxpr/htsd,hsd->hts/dot_general | solution.py:67
  325.9 3.6 multiply_multiply_fusion.2
  329.6 30.8 %fusion.122 = f32[8,64,1,64]{3,2,1,0:T(1,128)S(1)} fusion(f32[8,64,64,128]{3,2,1,0:T(8,128)S(1)} %multiply_multiply_fusion.2, f32[8,64,128,1]{2,0,1,3:T(8,128)S(1)} %get-tuple-element.728), kind=kOutput, calls=%fused_computation.29.clone.1 | convolution fusion | flops 50331648 | bytes 17170432 | tf_op jit(solution)/shard_map/while/body/eval_jaxpr/htsd,hsd->hts/dot_general | solution.py:67
  367.0 3.6 multiply_multiply_fusion.2
  370.6 30.8 %fusion.122 = f32[8,64,1,64]{3,2,1,0:T(1,128)S(1)} fusion(f32[8,64,64,128]{3,2,1,0:T(8,128)S(1)} %multiply_multiply_fusion.2, f32[8,64,128,1]{2,0,1,3:T(8,128)S(1)} %get-tuple-element.728), kind=kOutput, calls=%fused_computation.29.clone.1 | convolution fusion | flops 50331648 | bytes 17170432 | tf_op jit(solution)/shard_map/while/body/eval_jaxpr/htsd,hsd->hts/dot_general | solution.py:67
  408.1 3.6 multiply_multiply_fusion.2
  411.7 30.8 %fusion.122 = f32[8,64,1,64]{3,2,1,0:T(1,128)S(1)} fusion(f32[8,64,64,128]{3,2,1,0:T(8,128)S(1)} %multiply_multiply_fusion.2, f32[8,64,128,1]{2,0,1,3:T(8,128)S(1)} %get-tuple-element.728), kind=kOutput, calls=%fused_computation.29.clone.1 | convolution fusion | flops 50331648 | bytes 17170432 | tf_op jit(solution)/shard_map/while/body/eval_jaxpr/htsd,hsd->hts/dot_general | solution.py:67
  452.1 3.3 split.8
  455.4 4.1 copy.90
  461.2 7.4 %while.43 = (s32[]{:T(128)}, f32[8,256]{1,0:T(8,128)S(1)}, f32[8,256]{1,0:T(8,128)S(1)}, f32[8,256,64]{1,2,0:T(8,128)S(1)}, s32[]{:T(128)}, /*index=5*/bf16[4096...) while((s32[]{:T(128)}, f32[8,256]{1,0:T(8,128)S(1)}, ...), condition=%wide.region_17.18_spmd, body=%wide.region_12.17_spmd.sunk | while | flops 307962368 | bytes 15733113 | solution.py:268
  461.2 6.7 %conditional.2 = ((f32[8,256]{1,0:T(8,128)S(1)}, f32[8,256]{1,0:T(8,128)S(1)}, f32[8,256,64]{1,2,0:T(8,128)S(1)})) conditional(s32[]{:T(128)} %convert_element_type.125, (f32[8,256]{1,0:T(8,128)S(1)}, f32[8,256]{1,0:T(8,128)S(1)}, f32[8,256,64]{1,2,0:T(8,128)S(1)}) %tuple.104, (s32[]{:T(128)}, s32[]{:T(128)}, bf16[4096,256]{1,0:T(8,128)(2,1)}, ...), branch_computations={%region_13.13_spmd, %region_14.16_spmd} | conditional | flops 307962368 | bytes 15732850 | solution.py:250
  481.4 139.4 %all_gather.35 = f32[16,8,128]{2,1,0:T(8,128)S(1)} all-gather(f32[1,8,128]{2,1,0:T(8,128)S(1)} %exp.49), channel_id=1, replica_groups=mesh['sp'=16,'tp'=2] {'sp'}, dimensions={0}, use_global_device_ids=true | all-gather | bytes 69632 | tf_op jit(solution)/shard_map/all_gather | solution.py:25
  620.8 3.0 copy_multiply_fusion
  623.8 3.0 multiply_reduce_fusion
  630.1 24.3 %reduce-scatter.2.cloned.1.call-done = bf16[128,2048]{1,0:T(8,128)(2,1)} async-done(((bf16[256,2048]{1,0:T(8,128)(2,1)}), bf16[128,2048]{1,0:T(8,128)(2,1)}) %reduce-scatter.2.cloned.1.call-update) | async-done | bytes 524304 | tf_op jit(solution)/shard_map/reduce_scatter | solution.py:271
  (179 shorter events, 87.8 us)
Async XLA Ops:
  6.5 621.8 %copy-start = (bf16[512,2048]{1,0:T(8,128)(2,1)S(1)}, bf16[512,2048]{1,0:T(8,128)(2,1)}, u32[]{:S(2)}) copy-start(bf16[512,2048]{1,0:T(8,128)(2,1)} %param.43) | copy-start | bytes 6291460
  6.5 14.1 %all-gather.14.cloned.1.call-start = ((), (), s32[]{:S(2)}) async-start(), calls=%async_computation.4 | async-start | bytes 1572864 | tf_op jit(solution)/shard_map/all_gather | solution.py:148
  7.3 93.0 %all-gather.8.cloned.1.call-start = ((), (), s32[]{:S(2)}) async-start(), calls=%async_computation.1 | async-start | bytes 4456448 | tf_op jit(solution)/shard_map/all_gather | solution.py:142
  8.0 169.2 %all-gather.10.cloned.1.call-start = ((), (), s32[]{:S(2)}) async-start(), calls=%async_computation.2 | async-start | bytes 4456448 | tf_op jit(solution)/shard_map/all_gather | solution.py:143
  8.7 245.3 %all-gather.12.cloned.1.call-start = ((), (), s32[]{:S(2)}) async-start(), calls=%async_computation.3 | async-start | bytes 4456448 | tf_op jit(solution)/shard_map/all_gather | solution.py:144
  9.3 442.8 %all-gather.16.cloned.1.call-start = ((), (), s32[]{:S(2)}) async-start(), calls=%async_computation.5 | async-start | bytes 2506752 | tf_op jit(solution)/shard_map/all_gather | solution.py:17
  12.9 266.7 %copy-start.9 = (f32[8,128]{1,0:T(8,128)}, f32[8,128]{1,0:T(8,128)S(1)}, u32[]{:S(2)}) copy-start(f32[8,128]{1,0:T(8,128)S(1)} %bitcast_negate_fusion) | copy-start | bytes 12292
  31.1 592.6 %all-gather.18.cloned.1.call-start = ((), (), s32[]{:S(2)}) async-start(), calls=%async_computation.7 | async-start | bytes 8912896 | tf_op jit(solution)/shard_map/all_gather | solution.py:25
  276.2 1.6 copy-start.4
  276.2 1.9 copy-start.5
  277.8 1.7 copy-start.11
  281.3 165.4 %copy-start.10 = (f32[8,128]{1,0:T(8,128)S(1)}, f32[8,128]{1,0:T(8,128)}, u32[]{:S(2)}) copy-start(f32[8,128]{1,0:T(8,128)} %copy-done.9) | copy-start | bytes 12292
  281.3 165.5 %copy-start.14 = (f32[512]{0:T(512)S(1)}, f32[512]{0:T(512)}, u32[]{:S(2)}) copy-start(f32[512]{0:T(512)} %param.36) | copy-start | bytes 6148
  281.3 165.6 %copy-start.12 = (f32[256]{0:T(256)S(1)}, f32[256]{0:T(256)}, u32[]{:S(2)}) copy-start(f32[256]{0:T(256)} %get-tuple-element.540) | copy-start | bytes 3076
  281.3 167.7 %copy-start.6 = (bf16[512,512]{1,0:T(8,128)(2,1)S(1)}, bf16[512,512]{1,0:T(8,128)(2,1)}, u32[]{:S(2)}) copy-start(bf16[512,512]{1,0:T(8,128)(2,1)} %param.38) | copy-start | bytes 1572868
  445.8 0.8 copy-start.1
  445.8 5.6 copy-start.7
  445.8 5.6 copy-start.8
  446.6 207.8 %reduce-scatter.2.cloned.1.call-start = ((), (), s32[]{:S(2)}) async-start(), calls=%async_computation.6 | async-start | bytes 1572864 | tf_op jit(solution)/shard_map/reduce_scatter | solution.py:271
  464.2 1.5 copy-start.3
  475.4 145.3 %copy-start.2 = (f32[256,1024]{0,1:T(8,128)S(1)}, f32[256,1024]{0,1:T(8,128)}, u32[]{:S(2)}) copy-start(f32[256,1024]{0,1:T(8,128)} %get-tuple-element.554) | copy-start | bytes 3145732
  623.8 3.1 copy-start.13
  623.8 3.2 copy-start.15
Sparse Core Ops, SparseCore 0:
  8.9 11.7 all-gather.13
  23.4 76.7 all-gather.7
  103.0 74.1 all-gather.9
  179.9 74.1 all-gather.11
  256.6 66.2 all-gather.15
  446.7 111.0 all-gather.17
  630.2 24.1 reduce-scatter.1
